TPU v7x, 32 devices: a whole 2x2x4 slice. The times are simulated.
32 devices in a mesh: sp: 4 (over y, core), dp: 8 (over z, x).
Axes of the slice: x: 2, y: 2, z: 4, core: 2. Of those that a mesh axis runs over, the one named last changes fastest.
Arguments:
- queries: bfloat16 [8, 704, 2048], P('dp', 'sp'), may hold values from -24 to 24, as said below
- keys: bfloat16 [8, 704, 256], P('dp', 'sp'), may hold values from -24 to 24, as said below
- tokens: bfloat16 [8, 704, 2304], P('dp', 'sp'), may hold values from -18 to 18
- w_value: bfloat16 [2304, 256], P('dp'), may hold values from -0.125 to 0.125
- q_gain: float32 [128], replicated, may hold values from 0.5 to 6, as said below
- k_gain: float32 [128], replicated, may hold values from 0.5 to 6, as said below
Outputs:
- attended: bfloat16 [8, 704, 2048], P('dp', 'sp')
Inputs may be any that keep to these rules, and one draw needn't show every extreme that they name: `queries`: real-valued projected query entries. `keys`: real-valued projected key entries. `q_gain`: positive gains. `k_gain`: positive gains.
All inputs are finite; a program needn't handle non-finite values.
Results may differ from a plain program's by a relative error of at most 0.0022.
The roundings to bfloat16 on the way count: a program that leaves them out, or rounds other values in their place, can miss the bound.
Values may be sent and summed in bfloat16 or wider, within the bound.
A program may use at most 64 MiB of HBM per device.

v0:
```python
import functools
import math

import jax
import jax.numpy as jnp
from jax import lax
from jax.experimental import pallas as pl
from jax.experimental.pallas import tpu as pltpu
from jax.sharding import PartitionSpec as P

HD = 128
QH = 16
KVH = 2
GRID_W = 64
GROUP = QH // KVH
epsilon = 1e-06
MESH = pl.DeviceIdType.MESH


def inner_size(n):
    size = 1
    while size * size * 4 <= n and n % (size * 2) == 0:
        size *= 2
    return size


def partner(index, d, n):
    if n & (n - 1):
        return (index + d) % n
    bit = 1
    while bit <= d:
        if d & bit:
            index = index + bit - 2 * bit * (index // bit % 2)
        bit *= 2
    return index


def kernel(
    n_sp, n_dp, q_hbm, k_hbm, tok_hbm, w_hbm, qg_hbm, kg_hbm, out_ref,
    q_in, k_in, tok, wbuf, kbuf, vbuf, qrot, prob, cos_ref, sin_ref, qg_ref, kg_ref,
    in_sem, w_z, w_x, w_recv, t_send, t_recv, k_send, k_recv, k_fwd, k_frecv, v_send, v_recv, v_fwd, v_frecv,
):
    rows = q_hbm.shape[0]
    depth = w_hbm.shape[0]
    n_x = inner_size(n_dp)
    n_z = n_dp // n_x
    n_y = n_sp // 2
    sp = lax.axis_index("sp")
    dp = lax.axis_index("dp")
    z, x = dp // n_x, dp % n_x
    y, c = sp // 2, sp % 2
    sib = y * 2 + (1 - c)

    def block(d):
        return wbuf.at[pl.ds(pl.multiple_of(d * depth, 16), depth), :]

    def token_part(core):
        return tok.at[pl.ds(pl.multiple_of(core * rows, 16), rows), :]

    z_peers = [partner(z, d, n_z) for d in range(1, n_z)]
    x_peers = [((x + d) % n_x) for d in range(1, n_x)]
    y_peers = [((y + d) % n_y) for d in range(1, n_y)]

    barrier = pltpu.get_barrier_semaphore()
    for zp in z_peers:
        pl.semaphore_signal(barrier, inc=1, device_id=(sp, zp * n_x + x), device_id_type=MESH)
    for xp in x_peers:
        pl.semaphore_signal(barrier, inc=1, device_id=(sp, z * n_x + xp), device_id_type=MESH)
    for yp in y_peers:
        pl.semaphore_signal(barrier, inc=1, device_id=(yp * 2 + c, dp), device_id_type=MESH)
    pl.semaphore_signal(barrier, inc=1, device_id=(sib, dp), device_id_type=MESH)

    w_mine = w_hbm.at[:, pl.ds(pl.multiple_of(c * HD, HD), HD)]
    loads = [
        pltpu.make_async_copy(src, dst, in_sem.at[i])
        for i, (src, dst) in enumerate(
            (
                (kg_hbm, kg_ref), (k_hbm, k_in), (w_mine, block(dp)), (tok_hbm, token_part(c)),
                (q_hbm, q_in), (qg_hbm, qg_ref),
            )
        )
    ]
    for load in loads:
        load.start()

    pending = []

    def remote(src, dst, send, recv, where):
        return pltpu.make_async_remote_copy(
            src_ref=src, dst_ref=dst, send_sem=send, recv_sem=recv, device_id=where, device_id_type=MESH
        )

    def send(*args):
        copy = remote(*args)
        copy.start()
        pending.append(copy)

    pos = sp * rows + lax.broadcasted_iota(jnp.int32, (rows, HD), 0)
    lane = lax.broadcasted_iota(jnp.int32, (rows, HD), 1)
    grid_row = pos // GRID_W
    coord = jnp.where(lane < HD // 2, grid_row, pos - grid_row * GRID_W).astype(jnp.float32)
    step = (lax.broadcasted_iota(jnp.int32, (1, HD), 1) % (HD // 4)).astype(jnp.float32)
    angles = coord * jnp.exp2(step * (-2.0 * math.log2(10000.0) / (HD // 2)))
    first = lane % (HD // 2) < HD // 4
    cos_ref[...] = jnp.cos(angles)
    sine = jnp.sin(angles)
    sin_ref[...] = jnp.where(first, -sine, sine)

    def norm_rot(u, gain):
        u = u.astype(jnp.float32)
        u = u * lax.rsqrt(jnp.mean(u * u, axis=-1, keepdims=True) + epsilon) * gain
        other = jnp.where(first, pltpu.roll(u, HD - HD // 4, 1), pltpu.roll(u, HD // 4, 1))
        return (u * cos_ref[...] + other * sin_ref[...]).astype(jnp.bfloat16)

    def at(ref, s):
        return ref.at[pl.ds(pl.multiple_of(s * rows, 16), rows), :]

    own = pl.ds(pl.multiple_of(sp * rows, 16), rows)
    loads[0].wait()
    loads[1].wait()
    for g in range(KVH):
        kbuf[own, g * HD:(g + 1) * HD] = norm_rot(k_in[:, g * HD:(g + 1) * HD], kg_ref[...])
    loads[2].wait()

    pl.semaphore_wait(barrier, n_z - 1 + n_x - 1 + n_y)
    for i, zp in enumerate(z_peers):
        send(block(dp), block(dp), w_z.at[i], w_recv.at[dp], (sp, zp * n_x + x))
    for i, xp in enumerate(x_peers):
        send(block(dp), block(dp), w_x.at[0, i], w_recv.at[dp], (sp, z * n_x + xp))
    for i, yp in enumerate(y_peers):
        send(at(kbuf, sp), at(kbuf, sp), k_send.at[i], k_recv.at[y], (yp * 2 + c, dp))
    send(at(kbuf, sp), at(kbuf, sp), k_send.at[n_y - 1], k_frecv.at[y], (sib, dp))
    loads[3].wait()
    send(token_part(c), token_part(c), t_send.at[0], t_recv.at[0], (sib, dp))

    loads[4].wait()
    loads[5].wait()
    for h in range(QH):
        qrot[h] = norm_rot(q_in[:, h * HD:(h + 1) * HD], qg_ref[...])

    def arrived(d):
        remote(block(d), block(d), w_z.at[0], w_recv.at[d], (sp, d)).wait_recv()

    def relay(i):
        d = z_peers[i] * n_x + x
        arrived(d)
        for k, xp in enumerate(x_peers):
            send(block(d), block(d), w_x.at[i + 1, k], w_recv.at[d], (sp, z * n_x + xp))

    relays = [functools.partial(relay, i) for i in range(n_z - 1)]
    for i, yp in enumerate(y_peers):
        j = yp * 2 + c
        remote(at(kbuf, j), at(kbuf, j), k_send.at[0], k_recv.at[yp], (j, dp)).wait_recv()
        send(at(kbuf, j), at(kbuf, j), k_fwd.at[i], k_frecv.at[yp], (sib, dp))
    for step_on in relays[:1]:
        step_on()
    for yp in [y] + y_peers:
        j = yp * 2 + 1 - c
        remote(at(kbuf, j), at(kbuf, j), k_send.at[0], k_frecv.at[yp], (sib, dp)).wait_recv()

    scale = HD ** -0.5 * math.log2(math.e)

    def weights(h, g):
        s = lax.dot_general(
            qrot[h], kbuf[:, g * HD:(g + 1) * HD], (((1,), (1,)), ((), ())),
            preferred_element_type=jnp.float32,
        )
        e = jnp.exp2((s - jnp.max(s, axis=-1, keepdims=True)) * scale)
        prob[h] = (e * (1.0 / jnp.sum(e, axis=-1, keepdims=True))).astype(jnp.bfloat16)

    relays = relays[1:]
    done = 0
    for part in range(GROUP // 2):
        count = len(relays) * part // (GROUP // 2 - 1) if part != 1 else -(-len(relays) // 2)
        for step_on in relays[done:count]:
            step_on()
        done = count
        for g in range(KVH):
            base = g * GROUP + part * 2

            @pl.loop(base, base + 2)
            def _(h, g=g):
                weights(h, g)

    for zz in [z] + z_peers:
        for xp in x_peers:
            arrived(zz * n_x + xp)
    theirs = token_part(1 - c)
    remote(theirs, theirs, t_send.at[0], t_recv.at[0], (sib, dp)).wait_recv()

    def chip(head, yy):
        return vbuf.at[head, pl.ds(pl.multiple_of(yy * 2 * rows, 16), 2 * rows), :]

    chip(c, y)[...] = jnp.dot(tok[...], wbuf[...], preferred_element_type=jnp.float32).astype(jnp.bfloat16)
    for i, yp in enumerate(y_peers):
        send(chip(c, y), chip(c, y), v_send.at[i], v_recv.at[y], (yp * 2 + c, dp))
    send(chip(c, y), chip(c, y), v_send.at[n_y - 1], v_frecv.at[y], (sib, dp))
    for i, yp in enumerate(y_peers):
        there = chip(c, yp)
        remote(there, there, v_send.at[0], v_recv.at[yp], (yp * 2 + c, dp)).wait_recv()
        send(there, there, v_fwd.at[i], v_frecv.at[yp], (sib, dp))

    def attend(core):
        for i in range(GROUP):
            h = core * GROUP + i
            out_ref[:, pl.ds(pl.multiple_of(h * HD, HD), HD)] = jnp.dot(
                prob[h], vbuf[core], preferred_element_type=jnp.float32
            ).astype(jnp.bfloat16)

    attend(c)
    for yp in [y] + y_peers:
        there = chip(1 - c, yp)
        remote(there, there, v_send.at[0], v_frecv.at[yp], (sib, dp)).wait_recv()
    attend(1 - c)
    for copy in pending:
        copy.wait_send()


def per_device(queries, keys, tokens, w_value, q_gain, k_gain):
    n_sp, n_dp = lax.axis_size("sp"), lax.axis_size("dp")
    n_x = inner_size(n_dp)
    n_z = n_dp // n_x
    n_y = n_sp // 2
    rows, width = tokens.shape[1:]
    depth = w_value.shape[0]
    any_spec = pl.BlockSpec(memory_space=pltpu.HBM)
    bf16, f32 = jnp.bfloat16, jnp.float32
    dma = pltpu.SemaphoreType.DMA
    length = rows * n_sp
    buffers = [
        ((rows, QH * HD), bf16),
        ((rows, KVH * HD), bf16),
        ((2 * rows, width), bf16),
        ((width, HD), bf16),
        ((length, KVH * HD), bf16),
        ((KVH, length, HD), bf16),
        ((QH, rows, HD), bf16),
        ((QH, rows, length), bf16),
        ((rows, HD), f32),
        ((rows, HD), f32),
        ((1, HD), f32),
        ((1, HD), f32),
    ]
    held = sum(math.prod(shape) * jnp.dtype(kind).itemsize for shape, kind in buffers)
    limit = min(60 * 2 ** 20, held + held // 4 + 8 * rows * length * 4 + 4 * 2 ** 20)
    operands = (queries[0], keys[0], tokens[0], w_value, q_gain[None], k_gain[None])
    operands = [pltpu.with_memory_space_constraint(a, pltpu.HBM) for a in operands]
    out = pl.pallas_call(
        functools.partial(kernel, n_sp, n_dp),
        out_shape=jax.ShapeDtypeStruct((rows, QH * HD), bf16),
        in_specs=[any_spec] * 6,
        out_specs=pl.BlockSpec(memory_space=pltpu.VMEM),
        scratch_shapes=[pltpu.VMEM(shape, kind) for shape, kind in buffers]
        + [
            dma((6,)),
            dma((n_z,)),
            dma((n_z, n_x)),
            dma((n_dp,)),
            dma((1,)),
            dma((1,)),
            dma((n_y,)),
            dma((n_y,)),
            dma((n_y,)),
            dma((n_y,)),
            dma((n_y,)),
            dma((n_y,)),
            dma((n_y,)),
            dma((n_y,)),
        ],
        compiler_params=pltpu.CompilerParams(
            collective_id=0, has_side_effects=True, vmem_limit_bytes=limit
        ),
        name="fused_attention",
    )(*operands)
    return out[None]


def solution(mesh):
    in_specs = (
        P("dp", "sp", None),
        P("dp", "sp", None),
        P("dp", "sp", None),
        P("dp", None),
        P(),
        P(),
    )
    return jax.shard_map(
        per_device, mesh=mesh, in_specs=in_specs, out_specs=P("dp", "sp", None), check_vma=False
    )
```

profile of v0, /device:TPU:0, one launch (start us, length us, event | category | flops | bytes accessed | tf_op | source)
XLA Modules:
  0.0 27.0 jit_solution(11923924750088920135)
XLA Ops:
  0.0 26.1 %fused_attention.1 = bf16[176,2048]{1,0:T(8,128)(2,1)S(1)} custom-call(bf16[176,2048]{1,0:T(8,128)(2,1)} %bitcast.8, bf16[176,256]{1,0:T(8,128)(2,1)} %bitcast.9, bf16[176,2304]{1,0:T(8,128)(2,1)} %bitcast.7, bf16[288,256]{1,0:T(8,128)(2,1)} %w_hbm.1, f32[1,128]{1,0:T(1,128)} %bitcast.10, f32[1,128]{1,0:T(1,128)} %bitcast.11), custom_call_target="tpu_custom_call" | custom-call | tf_op jit(solution)/shard_map/fused_attention/pallas_call | solution.py:248
  26.1 0.9 %copy.8 = bf16[1,176,2048]{2,1,0:T(8,128)(2,1)} copy(bf16[1,176,2048]{2,1,0:T(8,128)(2,1)S(1)} %bitcast.6) | data formatting | bytes 1441792
where the time goes:
time: 27.1 us; the launch traced here: 27 us
  Pallas kernels  26.1 us (96%)
  local copies, waits for them, and re-layouts  0.86 us (3%)
    pallas_call x1, Pallas kernels, per_device(): pl.pallas_call(functools.partial(kernel, n_sp, n_dp), out_shape=jax.Shape...  26.1 us
    unnamed x1, local copies, waits for them, and re-layouts  0.86 us

commit v1 on v0

v1 whole, which is shorter than its diff:
```python
import functools
import math

import jax
import jax.numpy as jnp
from jax import lax
from jax.experimental import pallas as pl
from jax.experimental.pallas import tpu as pltpu
from jax.sharding import PartitionSpec as P

HD = 128
QH = 16
KVH = 2
GRID_W = 64
GROUP = QH // KVH
epsilon = 1e-06
MESH = pl.DeviceIdType.MESH


def inner_size(n):
    size = 1
    while size * size * 4 <= n and n % (size * 2) == 0:
        size *= 2
    return size


def partner(index, d, n):
    if n & (n - 1):
        return (index + d) % n
    bit = 1
    while bit <= d:
        if d & bit:
            index = index + bit - 2 * bit * (index // bit % 2)
        bit *= 2
    return index


def kernel(
    n_sp, n_dp, q_hbm, k_hbm, tok_hbm, w_hbm, qg_hbm, kg_hbm, out_ref,
    q_in, k_in, tok, wbuf, kbuf, vbuf, qrot, prob, cos_ref, sin_ref, cosg_ref, sing_ref, perm_ref, qg_ref, kg_ref,
    in_sem, w_z, w_x, w_d, w_recv, t_send, t_recv, k_send, k_recv, k_fwd, k_frecv, v_send, v_recv, v_fwd, v_frecv,
):
    rows = q_hbm.shape[0]
    depth = w_hbm.shape[0]
    length = kbuf.shape[0]
    n_x = inner_size(n_dp)
    n_z = n_dp // n_x
    n_y = n_sp // 2
    sp = lax.axis_index("sp")
    dp = lax.axis_index("dp")
    z, x = dp // n_x, dp % n_x
    y, c = sp // 2, sp % 2
    sib = y * 2 + (1 - c)

    def block(d):
        return wbuf.at[pl.ds(pl.multiple_of(d * depth, 16), depth), :]

    def token_part(core):
        return tok.at[pl.ds(pl.multiple_of(core * rows, 16), rows), :]

    z_peers = [partner(z, d, n_z) for d in range(1, n_z)]
    x_peers = [((x + d) % n_x) for d in range(1, n_x)]
    y_peers = [((y + d) % n_y) for d in range(1, n_y)]
    back = 0 if n_z & (n_z - 1) == 0 else n_z - 2
    diagonal = sorted({0, back}) if n_z > 1 else []

    with jax.named_scope("signal"):
        barrier = pltpu.get_barrier_semaphore()
        for zp in z_peers:
            pl.semaphore_signal(barrier, inc=1, device_id=(sp, zp * n_x + x), device_id_type=MESH)
        for xp in x_peers:
            pl.semaphore_signal(barrier, inc=1, device_id=(sp, z * n_x + xp), device_id_type=MESH)
            for i in diagonal:
                pl.semaphore_signal(barrier, inc=1, device_id=(sp, z_peers[i] * n_x + xp), device_id_type=MESH)
        for yp in y_peers:
            pl.semaphore_signal(barrier, inc=1, device_id=(yp * 2 + c, dp), device_id_type=MESH)
        pl.semaphore_signal(barrier, inc=1, device_id=(sib, dp), device_id_type=MESH)

        w_mine = w_hbm.at[:, pl.ds(pl.multiple_of(c * HD, HD), HD)]
        loads = [
            pltpu.make_async_copy(src, dst, in_sem.at[i])
            for i, (src, dst) in enumerate(
                (
                    (w_mine, block(dp)), (k_hbm, k_in), (kg_hbm, kg_ref), (tok_hbm, token_part(c)),
                    (q_hbm, q_in), (qg_hbm, qg_ref),
                )
            )
        ]
        for load in loads:
            load.start()

    pending = []

    def remote(src, dst, send, recv, where):
        return pltpu.make_async_remote_copy(
            src_ref=src, dst_ref=dst, send_sem=send, recv_sem=recv, device_id=where, device_id_type=MESH
        )

    def send(*args):
        copy = remote(*args)
        copy.start()
        pending.append(copy)

    with jax.named_scope("w_send"):
        loads[0].wait()
        pl.semaphore_wait(barrier, n_z - 1 + (n_x - 1) * (1 + len(diagonal)) + n_y)
        for k, xp in enumerate(x_peers):
            send(block(dp), block(dp), w_x.at[0, k], w_recv.at[dp], (sp, z * n_x + xp))
        for i, zp in enumerate(z_peers):
            send(block(dp), block(dp), w_z.at[i], w_recv.at[dp], (sp, zp * n_x + x))
        if n_z > 1:
            for k, xp in enumerate(x_peers):
                send(block(dp), block(dp), w_d.at[k], w_recv.at[dp], (sp, z_peers[0] * n_x + xp))

    with jax.named_scope("tables"):
        pos = sp * rows + lax.broadcasted_iota(jnp.int32, (rows, HD), 0)
        lane = lax.broadcasted_iota(jnp.int32, (rows, HD), 1)
        grid_row = pos // GRID_W
        coord = jnp.where(lane < HD // 2, grid_row, pos - grid_row * GRID_W).astype(jnp.float32)
        step = (lax.broadcasted_iota(jnp.int32, (1, HD), 1) % (HD // 4)).astype(jnp.float32)
        angles = coord * jnp.exp2(step * (-2.0 * math.log2(10000.0) / (HD // 2)))
        cos_ref[...] = jnp.cos(angles)
        sine = jnp.sin(angles)
        sin_ref[...] = jnp.where(lane % (HD // 2) < HD // 4, -sine, sine)
        source = lax.broadcasted_iota(jnp.int32, perm_ref.shape, 0)
        target = lax.broadcasted_iota(jnp.int32, perm_ref.shape, 1)
        swapped = jnp.where(target % (HD // 2) < HD // 4, target + HD // 4, target - HD // 4)
        perm_ref[...] = (source == swapped).astype(jnp.float32).astype(jnp.bfloat16)

    def gained(gain_ref):
        gain = gain_ref[...]
        wide = jnp.broadcast_to(gain, (8, HD))
        lanes = lax.broadcasted_iota(jnp.int32, (8, HD), 1)
        other = jnp.where(
            lanes % (HD // 2) < HD // 4, pltpu.roll(wide, HD - HD // 4, 1), pltpu.roll(wide, HD // 4, 1)
        )[:1]
        cosg_ref[...] = cos_ref[...] * gain
        sing_ref[...] = sin_ref[...] * other

    def norm_rot(pair):
        other = jnp.dot(pair, perm_ref[...], preferred_element_type=jnp.float32)
        heads = []
        for j in range(2):
            u = pair[:, j * HD:(j + 1) * HD].astype(jnp.float32)
            inverse = lax.rsqrt(jnp.mean(u * u, axis=-1, keepdims=True) + epsilon)
            turned = u * cosg_ref[...] + other[:, j * HD:(j + 1) * HD] * sing_ref[...]
            heads.append((turned * inverse).astype(jnp.bfloat16))
        return heads

    def at(ref, s):
        return ref.at[pl.ds(pl.multiple_of(s * rows, 16), rows), :]

    own = pl.ds(pl.multiple_of(sp * rows, 16), rows)
    with jax.named_scope("k_norm"):
        loads[1].wait()
        loads[2].wait()
        gained(kg_ref)
        for g, head in enumerate(norm_rot(k_in[...])):
            kbuf[own, g * HD:(g + 1) * HD] = head

    with jax.named_scope("k_send"):
        for i, yp in enumerate(y_peers):
            send(at(kbuf, sp), at(kbuf, sp), k_send.at[i], k_recv.at[y], (yp * 2 + c, dp))
        send(at(kbuf, sp), at(kbuf, sp), k_send.at[n_y - 1], k_frecv.at[y], (sib, dp))
        loads[3].wait()
        send(token_part(c), token_part(c), t_send.at[0], t_recv.at[0], (sib, dp))

    with jax.named_scope("q_norm"):
        loads[4].wait()
        loads[5].wait()
        gained(qg_ref)
        for b in range(QH // 2):
            for j, head in enumerate(norm_rot(q_in[:, 2 * b * HD:(2 * b + 2) * HD])):
                g, i = divmod(2 * b + j, GROUP)
                qrot[g, i * rows:(i + 1) * rows] = head

    def arrived(d):
        remote(block(d), block(d), w_z.at[0], w_recv.at[d], (sp, d)).wait_recv()

    def relay(i):
        d = z_peers[i] * n_x + x
        arrived(d)
        if i != back:
            for k, xp in enumerate(x_peers):
                send(block(d), block(d), w_x.at[i + 1, k], w_recv.at[d], (sp, z * n_x + xp))

    order = [i for i in range(n_z - 1) if i != back]
    order = order[::-1]
    scale = HD ** -0.5 * math.log2(math.e)

    def weights(g, start, size):
        s = lax.dot_general(
            kbuf[:, g * HD:(g + 1) * HD], qrot[g, start:start + size], (((1,), (1,)), ((), ())),
            preferred_element_type=jnp.float32,
        )
        e = jnp.exp2((s - jnp.max(s, axis=0, keepdims=True)) * scale)
        r = 1.0 / jnp.sum(e, axis=0, keepdims=True)
        prob[g, :, start:start + size] = (e * r).astype(jnp.bfloat16)

    half = len(order) // 2
    with jax.named_scope("relay0"):
        for i in order[:half]:
            relay(i)
    with jax.named_scope("k_relay"):
        for i, yp in enumerate(y_peers):
            j = yp * 2 + c
            remote(at(kbuf, j), at(kbuf, j), k_send.at[0], k_recv.at[yp], (j, dp)).wait_recv()
            send(at(kbuf, j), at(kbuf, j), k_fwd.at[i], k_frecv.at[yp], (sib, dp))
    with jax.named_scope("relay1"):
        for i in order[half:]:
            relay(i)
    with jax.named_scope("k_wait"):
        for yp in [y] + y_peers:
            j = yp * 2 + 1 - c
            remote(at(kbuf, j), at(kbuf, j), k_send.at[0], k_frecv.at[yp], (sib, dp)).wait_recv()
    for g in range(KVH):
        with jax.named_scope("scores"):
            weights(g, 0, GROUP * rows)

    with jax.named_scope("w_wait"):
        if n_z > 1:
            relay(back)
        for zz in [z] + z_peers:
            for xp in x_peers:
                arrived(zz * n_x + xp)
        theirs = token_part(1 - c)
        remote(theirs, theirs, t_send.at[0], t_recv.at[0], (sib, dp)).wait_recv()

    def part(head, yy, core):
        return vbuf.at[head, pl.ds(pl.multiple_of((yy * 2 + core) * rows, 16), rows), :]

    for core in range(2):
        with jax.named_scope("vproj"):
            mine = part(c, y, core)
            mine[...] = jnp.dot(
                tok[core * rows:(core + 1) * rows], wbuf[...], preferred_element_type=jnp.float32
            ).astype(jnp.bfloat16)
            for i, yp in enumerate(y_peers):
                send(mine, mine, v_send.at[core, i], v_recv.at[core, y], (yp * 2 + c, dp))
            send(mine, mine, v_send.at[core, n_y - 1], v_frecv.at[core, y], (sib, dp))
    with jax.named_scope("v_exch"):
        for core in range(2):
            for i, yp in enumerate(y_peers):
                there = part(c, yp, core)
                remote(there, there, v_send.at[0, 0], v_recv.at[core, yp], (yp * 2 + c, dp)).wait_recv()
                send(there, there, v_fwd.at[core, i], v_frecv.at[core, yp], (sib, dp))

    def attend(core):
        turned = lax.dot_general(
            vbuf[core], prob[core], (((0,), (0,)), ((), ())), preferred_element_type=jnp.float32
        )
        heads = turned.astype(jnp.bfloat16).T
        for i in range(GROUP):
            h = core * GROUP + i
            out_ref[:, pl.ds(pl.multiple_of(h * HD, HD), HD)] = heads[i * rows:(i + 1) * rows]

    with jax.named_scope("attend_c"):
        attend(c)
    with jax.named_scope("v_wait"):
        for core in range(2):
            for yp in [y] + y_peers:
                there = part(1 - c, yp, core)
                remote(there, there, v_send.at[0, 0], v_frecv.at[core, yp], (sib, dp)).wait_recv()
    with jax.named_scope("attend_o"):
        attend(1 - c)
    with jax.named_scope("wait_send"):
        for copy in pending:
            copy.wait_send()


def per_device(queries, keys, tokens, w_value, q_gain, k_gain):
    n_sp, n_dp = lax.axis_size("sp"), lax.axis_size("dp")
    n_x = inner_size(n_dp)
    n_z = n_dp // n_x
    n_y = n_sp // 2
    rows, width = tokens.shape[1:]
    depth = w_value.shape[0]
    any_spec = pl.BlockSpec(memory_space=pltpu.HBM)
    bf16, f32 = jnp.bfloat16, jnp.float32
    dma = pltpu.SemaphoreType.DMA
    length = rows * n_sp
    buffers = [
        ((rows, QH * HD), bf16),
        ((rows, KVH * HD), bf16),
        ((2 * rows, width), bf16),
        ((width, HD), bf16),
        ((length, KVH * HD), bf16),
        ((KVH, length, HD), bf16),
        ((KVH, GROUP * rows, HD), bf16),
        ((KVH, length, GROUP * rows), bf16),
        ((rows, HD), f32),
        ((rows, HD), f32),
        ((rows, HD), f32),
        ((rows, HD), f32),
        ((2 * HD, 2 * HD), bf16),
        ((1, HD), f32),
        ((1, HD), f32),
    ]
    held = sum(math.prod(shape) * jnp.dtype(kind).itemsize for shape, kind in buffers)
    limit = min(60 * 2 ** 20, held + held // 4 + 8 * rows * length * 4 + 4 * 2 ** 20)
    operands = (queries[0], keys[0], tokens[0], w_value, q_gain[None], k_gain[None])
    operands = [pltpu.with_memory_space_constraint(a, pltpu.HBM) for a in operands]
    out = pl.pallas_call(
        functools.partial(kernel, n_sp, n_dp),
        out_shape=jax.ShapeDtypeStruct((rows, QH * HD), bf16),
        in_specs=[any_spec] * 6,
        out_specs=pl.BlockSpec(memory_space=pltpu.VMEM),
        scratch_shapes=[pltpu.VMEM(shape, kind) for shape, kind in buffers]
        + [
            dma((6,)),
            dma((n_z,)),
            dma((n_z, n_x)),
            dma((n_x,)),
            dma((n_dp,)),
            dma((1,)),
            dma((1,)),
            dma((n_y,)),
            dma((n_y,)),
            dma((n_y,)),
            dma((n_y,)),
            dma((2, n_y)),
            dma((2, n_y)),
            dma((2, n_y)),
            dma((2, n_y)),
        ],
        compiler_params=pltpu.CompilerParams(
            collective_id=0, has_side_effects=True, vmem_limit_bytes=limit
        ),
        name="fused_attention",
    )(*operands)
    return out[None]


def solution(mesh):
    in_specs = (
        P("dp", "sp", None),
        P("dp", "sp", None),
        P("dp", "sp", None),
        P("dp", None),
        P(),
        P(),
    )
    return jax.shard_map(
        per_device, mesh=mesh, in_specs=in_specs, out_specs=P("dp", "sp", None), check_vma=False
    )
```

time: 27.1 us -> 24.2 us (0.89)
  Pallas kernels: 26.1 us -> 23.1 us
    pallas_call x1, Pallas kernels: 26.1 us -> 23.1 us  [per_device(): pl.pallas_call(functools.partial(kernel, n_sp, n_dp), out_shape=jax.Shape...]
where the time goes in v1:
time: 24.2 us; the launch traced here: 23.9 us
  Pallas kernels  23.1 us (95%)
  local copies, waits for them, and re-layouts  0.86 us (4%)
    pallas_call x1, Pallas kernels, per_device(): pl.pallas_call(functools.partial(kernel, n_sp, n_dp), out_shape=jax.Shape...  23.1 us
    unnamed x1, local copies, waits for them, and re-layouts  0.86 us

profile of v1, /device:TPU:0, one launch (start us, length us, event | category | flops | bytes accessed | tf_op | source)
XLA Modules:
  0.0 23.9 jit_solution(5506206834261377455)
XLA Ops:
  0.0 23.1 %fused_attention.1 = bf16[176,2048]{1,0:T(8,128)(2,1)S(1)} custom-call(bf16[176,2048]{1,0:T(8,128)(2,1)} %bitcast.8, bf16[176,256]{1,0:T(8,128)(2,1)} %bitcast.9, bf16[176,2304]{1,0:T(8,128)(2,1)} %bitcast.7, bf16[288,256]{1,0:T(8,128)(2,1)} %w_hbm.1, f32[1,128]{1,0:T(1,128)} %bitcast.10, f32[1,128]{1,0:T(1,128)} %bitcast.11), custom_call_target="tpu_custom_call" | custom-call | tf_op jit(solution)/shard_map/fused_attention/pallas_call | solution.py:303
  23.1 0.9 %copy.8 = bf16[1,176,2048]{2,1,0:T(8,128)(2,1)} copy(bf16[1,176,2048]{2,1,0:T(8,128)(2,1)S(1)} %bitcast.6) | data formatting | bytes 1441792

commit v2 on v1

--- a/solution.py
+++ b/solution.py
@@ -38,10 +38,11 @@
 def kernel(
     n_sp, n_dp, q_hbm, k_hbm, tok_hbm, w_hbm, qg_hbm, kg_hbm, out_ref,
     q_in, k_in, tok, wbuf, kbuf, vbuf, qrot, prob, cos_ref, sin_ref, cosg_ref, sing_ref, perm_ref, qg_ref, kg_ref,
-    in_sem, w_z, w_x, w_d, w_recv, t_send, t_recv, k_send, k_recv, k_fwd, k_frecv, v_send, v_recv, v_fwd, v_frecv,
+    v_acc, in_sem, w_z, w_x, w_d, w_recv, h_send, h_recv, t_send, t_recv, k_send, k_recv, k_fwd, k_frecv, v_send, v_recv, v_fwd, v_frecv,
 ):
     rows = q_hbm.shape[0]
     depth = w_hbm.shape[0]
+    width = tok_hbm.shape[1]
     length = kbuf.shape[0]
     n_x = inner_size(n_dp)
     n_z = n_dp // n_x
@@ -55,6 +56,9 @@
     def block(d):
         return wbuf.at[pl.ds(pl.multiple_of(d * depth, 16), depth), :]
 
+    def half(d, h):
+        return wbuf.at[pl.ds(pl.multiple_of(d * depth + h * (depth // 2), 16), depth // 2), :]
+
     def token_part(core):
         return tok.at[pl.ds(pl.multiple_of(core * rows, 16), rows), :]
 
@@ -63,18 +67,26 @@
     y_peers = [((y + d) % n_y) for d in range(1, n_y)]
     back = 0 if n_z & (n_z - 1) == 0 else n_z - 2
     diagonal = sorted({0, back}) if n_z > 1 else []
+    paired = (n_x, n_y, n_z) == (2, 2, 4) and depth % 32 == 0 and width % (4 * HD) == 0
+    corners = sorted(((i, j, k) for i in range(2) for j in range(2) for k in range(2) if i + j + k), key=sum)[::-1]
+
+    def corner(i, j, k):
+        return (x + i) % 2, (y + j) % 2, z + k - 2 * k * (z % 2)
+
+    def device(xx, yy, zz):
+        return (yy * 2 + c, zz * n_x + xx)
 
     with jax.named_scope("signal"):
         barrier = pltpu.get_barrier_semaphore()
-        for zp in z_peers:
-            pl.semaphore_signal(barrier, inc=1, device_id=(sp, zp * n_x + x), device_id_type=MESH)
-        for xp in x_peers:
-            pl.semaphore_signal(barrier, inc=1, device_id=(sp, z * n_x + xp), device_id_type=MESH)
-            for i in diagonal:
-                pl.semaphore_signal(barrier, inc=1, device_id=(sp, z_peers[i] * n_x + xp), device_id_type=MESH)
-        for yp in y_peers:
-            pl.semaphore_signal(barrier, inc=1, device_id=(yp * 2 + c, dp), device_id_type=MESH)
-        pl.semaphore_signal(barrier, inc=1, device_id=(sib, dp), device_id_type=MESH)
+        if paired:
+            greeted = [device(x, y, partner(z, 2, n_z))] + [device(*corner(*at)) for at in corners]
+        else:
+            greeted = [(sp, zp * n_x + x) for zp in z_peers] + [(sp, z * n_x + xp) for xp in x_peers]
+            greeted += [(sp, z_peers[i] * n_x + xp) for xp in x_peers for i in diagonal]
+            greeted += [(yp * 2 + c, dp) for yp in y_peers]
+        greeted.append((sib, dp))
+        for where in greeted:
+            pl.semaphore_signal(barrier, inc=1, device_id=where, device_id_type=MESH)
 
         w_mine = w_hbm.at[:, pl.ds(pl.multiple_of(c * HD, HD), HD)]
         loads = [
@@ -103,14 +115,20 @@
 
     with jax.named_scope("w_send"):
         loads[0].wait()
-        pl.semaphore_wait(barrier, n_z - 1 + (n_x - 1) * (1 + len(diagonal)) + n_y)
-        for k, xp in enumerate(x_peers):
-            send(block(dp), block(dp), w_x.at[0, k], w_recv.at[dp], (sp, z * n_x + xp))
-        for i, zp in enumerate(z_peers):
-            send(block(dp), block(dp), w_z.at[i], w_recv.at[dp], (sp, zp * n_x + x))
-        if n_z > 1:
+        pl.semaphore_wait(barrier, len(greeted))
+        if paired:
+            mine = half(dp, y)
+            send(mine, mine, h_send.at[7], h_recv.at[dp, y], device(x, y, partner(z, 2, n_z)))
+            for i, at in enumerate(((1, 0, 0), (0, 0, 1), (1, 0, 1))):
+                send(block(dp), block(dp), w_z.at[i], w_recv.at[dp], device(*corner(*at)))
+        else:
             for k, xp in enumerate(x_peers):
-                send(block(dp), block(dp), w_d.at[k], w_recv.at[dp], (sp, z_peers[0] * n_x + xp))
+                send(block(dp), block(dp), w_x.at[0, k], w_recv.at[dp], (sp, z * n_x + xp))
+            for i, zp in enumerate(z_peers):
+                send(block(dp), block(dp), w_z.at[i], w_recv.at[dp], (sp, zp * n_x + x))
+            if n_z > 1:
+                for k, xp in enumerate(x_peers):
+                    send(block(dp), block(dp), w_d.at[k], w_recv.at[dp], (sp, z_peers[0] * n_x + xp))
 
     with jax.named_scope("tables"):
         pos = sp * rows + lax.broadcasted_iota(jnp.int32, (rows, HD), 0)
@@ -147,7 +165,7 @@
             heads.append((turned * inverse).astype(jnp.bfloat16))
         return heads
 
-    def at(ref, s):
+    def rows_of(ref, s):
         return ref.at[pl.ds(pl.multiple_of(s * rows, 16), rows), :]
 
     own = pl.ds(pl.multiple_of(sp * rows, 16), rows)
@@ -160,8 +178,8 @@
 
     with jax.named_scope("k_send"):
         for i, yp in enumerate(y_peers):
-            send(at(kbuf, sp), at(kbuf, sp), k_send.at[i], k_recv.at[y], (yp * 2 + c, dp))
-        send(at(kbuf, sp), at(kbuf, sp), k_send.at[n_y - 1], k_frecv.at[y], (sib, dp))
+            send(rows_of(kbuf, sp), rows_of(kbuf, sp), k_send.at[i], k_recv.at[y], (yp * 2 + c, dp))
+        send(rows_of(kbuf, sp), rows_of(kbuf, sp), k_send.at[n_y - 1], k_frecv.at[y], (sib, dp))
         loads[3].wait()
         send(token_part(c), token_part(c), t_send.at[0], t_recv.at[0], (sib, dp))
 
@@ -184,8 +202,6 @@
             for k, xp in enumerate(x_peers):
                 send(block(d), block(d), w_x.at[i + 1, k], w_recv.at[d], (sp, z * n_x + xp))
 
-    order = [i for i in range(n_z - 1) if i != back]
-    order = order[::-1]
     scale = HD ** -0.5 * math.log2(math.e)
 
     def weights(g, start, size):
@@ -197,34 +213,61 @@
         r = 1.0 / jnp.sum(e, axis=0, keepdims=True)
         prob[g, :, start:start + size] = (e * r).astype(jnp.bfloat16)
 
-    half = len(order) // 2
-    with jax.named_scope("relay0"):
-        for i in order[:half]:
-            relay(i)
+    def half_arrived(d, h):
+        remote(half(d, h), half(d, h), h_send.at[0], h_recv.at[d, h], (sp, dp)).wait_recv()
+
+    with jax.named_scope("w_relay"):
+        if paired:
+            d = partner(z, 2, n_z) * n_x + x
+            half_arrived(d, y)
+            for i, at in enumerate(corners):
+                send(half(d, y), half(d, y), h_send.at[i], h_recv.at[d, y], device(*corner(*at)))
     with jax.named_scope("k_relay"):
         for i, yp in enumerate(y_peers):
             j = yp * 2 + c
-            remote(at(kbuf, j), at(kbuf, j), k_send.at[0], k_recv.at[yp], (j, dp)).wait_recv()
-            send(at(kbuf, j), at(kbuf, j), k_fwd.at[i], k_frecv.at[yp], (sib, dp))
-    with jax.named_scope("relay1"):
-        for i in order[half:]:
-            relay(i)
+            remote(rows_of(kbuf, j), rows_of(kbuf, j), k_send.at[0], k_recv.at[yp], (j, dp)).wait_recv()
+            send(rows_of(kbuf, j), rows_of(kbuf, j), k_fwd.at[i], k_frecv.at[yp], (sib, dp))
+    with jax.named_scope("w_relays"):
+        if not paired:
+            for i in range(n_z - 1):
+                if i != back:
+                    relay(i)
     with jax.named_scope("k_wait"):
         for yp in [y] + y_peers:
             j = yp * 2 + 1 - c
-            remote(at(kbuf, j), at(kbuf, j), k_send.at[0], k_frecv.at[yp], (sib, dp)).wait_recv()
+            remote(rows_of(kbuf, j), rows_of(kbuf, j), k_send.at[0], k_frecv.at[yp], (sib, dp)).wait_recv()
     for g in range(KVH):
         with jax.named_scope("scores"):
             weights(g, 0, GROUP * rows)
 
-    with jax.named_scope("w_wait"):
-        if n_z > 1:
-            relay(back)
-        for zz in [z] + z_peers:
-            for xp in x_peers:
-                arrived(zz * n_x + xp)
+    with jax.named_scope("t_wait"):
         theirs = token_part(1 - c)
         remote(theirs, theirs, t_send.at[0], t_recv.at[0], (sib, dp)).wait_recv()
+
+    def project(core, near):
+        part = (z // 2 + 1 - near) % 2 if paired else 0
+        span = pl.ds(pl.multiple_of(part * (width // 2), HD), width // 2) if paired else slice(None)
+        return jnp.dot(tok[core * rows:(core + 1) * rows, span], wbuf[span, :], preferred_element_type=jnp.float32)
+
+    if paired:
+        with jax.named_scope("w_near"):
+            for at in ((1, 0, 0), (0, 0, 1), (1, 0, 1)):
+                xx, _, zz = corner(*at)
+                arrived(zz * n_x + xx)
+        with jax.named_scope("vproj_near"):
+            for core in range(2):
+                v_acc[core * rows:(core + 1) * rows, :] = project(core, 1)
+        with jax.named_scope("w_wait"):
+            for at in corners:
+                xx, yy, zz = corner(*at)
+                half_arrived(partner(zz, 2, n_z) * n_x + xx, yy)
+    else:
+        with jax.named_scope("w_wait"):
+            if n_z > 1:
+                relay(back)
+            for zz in [z] + z_peers:
+                for xp in x_peers:
+                    arrived(zz * n_x + xp)
 
     def part(head, yy, core):
         return vbuf.at[head, pl.ds(pl.multiple_of((yy * 2 + core) * rows, 16), rows), :]
@@ -232,9 +275,10 @@
     for core in range(2):
         with jax.named_scope("vproj"):
             mine = part(c, y, core)
-            mine[...] = jnp.dot(
-                tok[core * rows:(core + 1) * rows], wbuf[...], preferred_element_type=jnp.float32
-            ).astype(jnp.bfloat16)
+            total = project(core, 0)
+            if paired:
+                total = total + v_acc[core * rows:(core + 1) * rows, :]
+            mine[...] = total.astype(jnp.bfloat16)
             for i, yp in enumerate(y_peers):
                 send(mine, mine, v_send.at[core, i], v_recv.at[core, y], (yp * 2 + c, dp))
             send(mine, mine, v_send.at[core, n_y - 1], v_frecv.at[core, y], (sib, dp))
@@ -295,6 +339,7 @@
         ((2 * HD, 2 * HD), bf16),
         ((1, HD), f32),
         ((1, HD), f32),
+        ((2 * rows, HD), f32),
     ]
     held = sum(math.prod(shape) * jnp.dtype(kind).itemsize for shape, kind in buffers)
     limit = min(60 * 2 ** 20, held + held // 4 + 8 * rows * length * 4 + 4 * 2 ** 20)
@@ -312,6 +357,8 @@
             dma((n_z, n_x)),
             dma((n_x,)),
             dma((n_dp,)),
+            dma((8,)),
+            dma((n_dp, 2)),
             dma((1,)),
             dma((1,)),
             dma((n_y,)),

time: 24.2 us -> 23.5 us (0.971)
  Pallas kernels: 23.1 us -> 22.3 us
    pallas_call x1, Pallas kernels: 23.1 us -> 22.3 us  [per_device(): pl.pallas_call(functools.partial(kernel, n_sp, n_dp), out_shape=jax.Shape...]
where the time goes in v2:
time: 23.5 us; the launch traced here: 23.2 us
  Pallas kernels  22.3 us (95%)
  local copies, waits for them, and re-layouts  0.86 us (4%)
    pallas_call x1, Pallas kernels, per_device(): pl.pallas_call(functools.partial(kernel, n_sp, n_dp), out_shape=jax.Shape...  22.3 us
    unnamed x1, local copies, waits for them, and re-layouts  0.86 us

profile of v2, /device:TPU:0, one launch (start us, length us, event | category | flops | bytes accessed | tf_op | source)
XLA Modules:
  0.0 23.2 jit_solution(6353068677749525646)
XLA Ops:
  0.0 22.3 %fused_attention.1 = bf16[176,2048]{1,0:T(8,128)(2,1)S(1)} custom-call(bf16[176,2048]{1,0:T(8,128)(2,1)} %bitcast.8, bf16[176,256]{1,0:T(8,128)(2,1)} %bitcast.9, bf16[176,2304]{1,0:T(8,128)(2,1)} %bitcast.7, bf16[288,256]{1,0:T(8,128)(2,1)} %w_hbm.1, f32[1,128]{1,0:T(1,128)} %bitcast.10, f32[1,128]{1,0:T(1,128)} %bitcast.11), custom_call_target="tpu_custom_call" | custom-call | tf_op jit(solution)/shard_map/fused_attention/pallas_call | solution.py:348
  22.3 0.9 %copy.8 = bf16[1,176,2048]{2,1,0:T(8,128)(2,1)} copy(bf16[1,176,2048]{2,1,0:T(8,128)(2,1)S(1)} %bitcast.6) | data formatting | bytes 1441792

commit v3 on v2

--- a/solution.py
+++ b/solution.py
@@ -67,7 +67,7 @@
     y_peers = [((y + d) % n_y) for d in range(1, n_y)]
     back = 0 if n_z & (n_z - 1) == 0 else n_z - 2
     diagonal = sorted({0, back}) if n_z > 1 else []
-    paired = (n_x, n_y, n_z) == (2, 2, 4) and depth % 32 == 0 and width % (4 * HD) == 0
+    paired = (n_x, n_y, n_z) == (2, 2, 4) and depth % 32 == 0 and width % (2 * HD) == 0
     corners = sorted(((i, j, k) for i in range(2) for j in range(2) for k in range(2) if i + j + k), key=sum)[::-1]
 
     def corner(i, j, k):

time: 23.5 us -> 21.1 us (0.90)
  Pallas kernels: 22.3 us -> 20 us
    pallas_call x1, Pallas kernels: 22.3 us -> 20 us  [per_device(): pl.pallas_call(functools.partial(kernel, n_sp, n_dp), out_shape=jax.Shape...]
where the time goes in v3:
time: 21.1 us; the launch traced here: 20.9 us
  Pallas kernels  20 us (95%)
  local copies, waits for them, and re-layouts  0.86 us (4%)
    pallas_call x1, Pallas kernels, per_device(): pl.pallas_call(functools.partial(kernel, n_sp, n_dp), out_shape=jax.Shape...  20 us
    unnamed x1, local copies, waits for them, and re-layouts  0.86 us

profile of v3, /device:TPU:0, one launch (start us, length us, event | category | flops | bytes accessed | tf_op | source)
XLA Modules:
  0.0 20.9 jit_solution(3085801138200924287)
XLA Ops:
  0.0 20.0 %fused_attention.1 = bf16[176,2048]{1,0:T(8,128)(2,1)S(1)} custom-call(bf16[176,2048]{1,0:T(8,128)(2,1)} %bitcast.8, bf16[176,256]{1,0:T(8,128)(2,1)} %bitcast.9, bf16[176,2304]{1,0:T(8,128)(2,1)} %bitcast.7, bf16[288,256]{1,0:T(8,128)(2,1)} %w_hbm.1, f32[1,128]{1,0:T(1,128)} %bitcast.10, f32[1,128]{1,0:T(1,128)} %bitcast.11), custom_call_target="tpu_custom_call" | custom-call | tf_op jit(solution)/shard_map/fused_attention/pallas_call | solution.py:348
  20.0 0.9 %copy.8 = bf16[1,176,2048]{2,1,0:T(8,128)(2,1)} copy(bf16[1,176,2048]{2,1,0:T(8,128)(2,1)S(1)} %bitcast.6) | data formatting | bytes 1441792
